TPU v7x, 512 devices: a whole 4x8x8 slice. The times are simulated.
512 devices in a mesh: kv: 128 (over z, y, core), tp: 4 (over x).
Axes of the slice: x: 4, y: 8, z: 8, core: 2. Of those that a mesh axis runs over, the one named last changes fastest.
Arguments:
- tokens: bfloat16 [8, 2048], P(None, 'kv'), may hold values from -6 to 6
- in_gain: float32 [2048], P('kv'), may hold values from 0.1 to 1.9
- w_query: bfloat16 [2048, 512], P('kv', 'tp'), may hold values from -0.125 to 0.125
- score_bias: float32 [4], P('tp'), as said below
- cache_keys: bfloat16 [8, 131072, 512], P(None, 'kv', 'tp'), may hold values from -8 to 8, as said below
- cache_values: bfloat16 [8, 131072, 512], P(None, 'kv', 'tp'), may hold values from -6 to 6
- lengths: int32 [8], replicated, may hold values from 16384 to 131072, as said below
- head_gain: float32 [512], P('tp'), may hold values from 0.1 to 1.9
- w_out: bfloat16 [512, 2048], P('tp', 'kv'), may hold values from -0.25 to 0.25
Outputs:
- mixed: bfloat16 [8, 2048], P(None, 'kv')
Inputs may be any that keep to these rules, and one draw needn't show every extreme that they name: `score_bias`: one value a head, added to every score of that head. `cache_keys`: real-valued key entries. `lengths`: one sequence has all 131072 positions cached.
All inputs are finite; a program needn't handle non-finite values.
Results may differ from a plain program's by a relative error of at most 0.0095.
The roundings to bfloat16 on the way count: a program that leaves them out, or rounds other values in their place, can miss the bound.
Values may be sent and summed in bfloat16 or wider, within the bound.
A program may use at most 64 MiB of HBM per device.

v0:
```python
import jax
import jax.numpy as jnp
from jax import lax
from jax.sharding import Mesh
from jax.sharding import PartitionSpec as P

D = 2048
KV = ("kv_0", "kv_1", "kv_2")


EPS = 1e-06


def one_axis_at_a_time(shard, axes):
    for axis in axes:
        shard = lax.psum(shard, axis)
    return shard


def neutral_like(shard, identity):
    return jnp.broadcast_to(jnp.asarray(identity, shard.dtype), shard.shape)


def entering(shard, axes, combine, identity):
    before = start = neutral_like(shard, identity)
    so_far = shard
    for axis in reversed(axes):
        length, place = (lax.axis_size(axis), lax.axis_index(axis))
        pieces = lax.all_gather(so_far, axis)
        inside, so_far = (start, start)
        for k in reversed(range(length)):
            passed = k > place
            so_far = combine(so_far, pieces[k])
            inside = jnp.where(passed, so_far, inside)
        before = combine(inside, before)
    return before


def copy_for_each(shard, axis):
    length = lax.axis_size(axis)
    return lax.all_to_all(
        jnp.broadcast_to(shard[None], (length, *shard.shape)), axis, 0, 0, tiled=True
    )


def over_copies(shard, axis):
    return copy_for_each(shard, axis).astype(jnp.float32).sum(axis=0)


def shards(
    tokens, in_gain, w_query, score_bias, cache_keys, cache_values, lengths, head_gain, w_out
):
    sequences = tokens.shape[0]
    local_len = cache_keys.shape[1]
    head_width = cache_keys.shape[2]
    heads_here = score_bias.shape[0]
    head_size = head_width // heads_here
    as_float = tokens.astype(jnp.float32)
    gained = (as_float * in_gain).astype(jnp.bfloat16)
    partial_value = jnp.dot(gained, w_query, preferred_element_type=jnp.float32)
    squares = jnp.sum(as_float * as_float, axis=1)
    summed, total_sq = (one_axis_at_a_time(partial_value, KV), one_axis_at_a_time(squares, KV))
    row_scale = lax.rsqrt(total_sq / D + EPS)
    queries = (
        (summed * row_scale[:, None]).astype(jnp.bfloat16).reshape(sequences, heads_here, head_size)
    )
    key_heads = cache_keys.reshape(sequences, local_len, heads_here, head_size)
    value_heads = cache_values.reshape(sequences, local_len, heads_here, head_size)
    scores = jnp.einsum("bhd,bphd->bhp", queries, key_heads, preferred_element_type=jnp.float32)
    scores = scores * head_size ** (-0.5) + score_bias[None, :, None]
    offset = lax.axis_index(KV) * local_len
    places = offset + lax.iota(jnp.int32, local_len)
    usable = places[None, None, :] < lengths[:, None, None]
    log_keep = jnp.where(usable, jax.nn.log_sigmoid(-scores), 0.0)
    strict_upper = (
        lax.iota(jnp.int32, local_len)[:, None] > lax.iota(jnp.int32, local_len)[None, :]
    ).astype(jnp.float32)
    suffix = jnp.einsum("bhr,rs->bhs", log_keep, strict_upper, precision=lax.Precision.HIGHEST)
    weights = jnp.where(usable, jnp.exp(jax.nn.log_sigmoid(scores) + suffix), 0.0).astype(
        jnp.bfloat16
    )
    local_out = jnp.einsum(
        "bhp,bphd->bhd", weights, value_heads, preferred_element_type=jnp.float32
    )
    seg_total = jnp.sum(log_keep, axis=2)
    later_sum = entering(seg_total, KV, jnp.add, jnp.zeros_like(seg_total))
    attended = one_axis_at_a_time(local_out * jnp.exp(later_sum)[..., None], KV)
    mean_sq = jnp.mean(attended * attended, axis=2)
    normed = attended * lax.rsqrt(mean_sq + EPS)[..., None]
    normed = (normed.reshape(sequences, head_width) * head_gain).astype(jnp.bfloat16)
    part_out = jnp.dot(normed, w_out, preferred_element_type=jnp.float32)
    return over_copies(part_out.astype(jnp.bfloat16), "tp").astype(jnp.float32).astype(jnp.bfloat16)


def solution(mesh):
    finer = Mesh(mesh.devices.reshape(8, 8, 2, mesh.shape["tp"]), ("kv_0", "kv_1", "kv_2", "tp"))
    placed = (
        P(None, KV),
        P(KV),
        P(KV, "tp"),
        P("tp"),
        P(None, KV, "tp"),
        P(None, KV, "tp"),
        P(),
        P("tp"),
        P("tp", KV),
    )
    return jax.shard_map(
        shards, mesh=finer, in_specs=placed, out_specs=P(None, KV), check_vma=False
    )
```

profile of v0, /device:TPU:1, one launch (start us, length us, event | category | flops | bytes accessed | tf_op | source)
XLA Modules:
  0.0 129.4 jit_solution(17400130725583646784)
XLA Ops:
  0.0 0.0 copy-start
  0.0 0.0 copy-start.1
  0.0 0.9 fusion.18
  1.0 0.8 fusion.24
  1.8 20.5 %all-reduce.3 = (f32[8,128]{1,0:T(8,128)S(1)}, f32[8]{0:T(128)S(1)}) all-reduce(f32[8,128]{1,0:T(8,128)S(1)} %fusion.24, f32[8]{0:T(128)S(1)} %fusion.18), channel_id=1, replica_groups=mesh['kv_0'=8,'kv_1'=8,'kv_2'=2,'tp'=4] {'kv_0'}, use_global_device_ids=true, to_apply=%region_0.0 | all-reduce | flops 1032 | bytes 8256 | tf_op jit(solution)/shard_map/psum | solution.py:16
  22.3 14.1 %all-reduce.2 = (f32[8,128]{1,0:T(8,128)S(1)}, f32[8]{0:T(128)S(1)}) all-reduce(f32[8,128]{1,0:T(8,128)S(1)} %get-tuple-element.7, f32[8]{0:T(128)S(1)} %get-tuple-element.8), channel_id=1, replica_groups=mesh['kv_0'=8,'kv_1'=8,'kv_2'=2,'tp'=4] {'kv_1'}, use_global_device_ids=true, to_apply=%region_1.0 | all-reduce | flops 1032 | bytes 8256 | tf_op jit(solution)/shard_map/psum | solution.py:16
  36.4 10.3 %all-reduce.4 = (f32[8,128]{1,0:T(8,128)S(1)}, f32[8]{0:T(128)S(1)}) all-reduce(f32[8,128]{1,0:T(8,128)S(1)} %get-tuple-element.5, f32[8]{0:T(128)S(1)} %get-tuple-element.6), channel_id=1, replica_groups=mesh['kv_0'=8,'kv_1'=8,'kv_2'=2,'tp'=4] {'kv_2'}, use_global_device_ids=true, to_apply=%region_2.0 | all-reduce | flops 1032 | bytes 8256 | tf_op jit(solution)/shard_map/psum | solution.py:16
  47.4 0.1 fusion.22
  47.5 0.0 copy-done
  47.5 0.6 fusion.20
  48.1 0.0 copy-start.2
  48.1 0.0 copy-start.3
  48.1 1.4 %dynamic-slice = u32[1]{0:T(128)} dynamic-slice(u32[512]{0:T(512)} %constant.62, u32[]{:T(128)S(6)} %add.303), dynamic_slice_sizes={1} | dynamic-slice | bytes 12
  50.2 0.0 copy-done.1
  50.2 0.2 fusion.11
  50.4 0.2 dynamic-update-slice
  50.6 2.5 %all-reduce = f32[16]{0:T(128)S(1)} all-reduce(f32[16]{0:T(128)S(1)} %dynamic-update-slice), channel_id=2, replica_groups=mesh['kv_0'=8,'kv_1'=8,'kv_2'=2,'tp'=4] {'kv_2'}, use_global_device_ids=true, to_apply=%add | all-reduce | flops 16 | bytes 128
  53.1 1.3 %dynamic-slice.1 = u32[1]{0:T(128)} dynamic-slice(u32[512]{0:T(512)} %constant.67, u32[]{:T(128)S(6)} %add.303), dynamic_slice_sizes={1} | dynamic-slice | bytes 12
  55.1 0.2 fusion.34
  55.3 11.2 %all-reduce.1 = f32[64]{0:T(128)S(1)} all-reduce(f32[64]{0:T(128)S(1)} %fusion.34), channel_id=3, replica_groups=mesh['kv_0'=8,'kv_1'=8,'kv_2'=2,'tp'=4] {'kv_1'}, use_global_device_ids=true, to_apply=%add.1 | all-reduce | flops 64 | bytes 512
  66.5 0.1 bitcast_add_fusion
  66.6 9.8 %all_gather.17 = f32[8,8,1]{1,2,0:T(1,128)S(1)} all-gather(f32[1,8,1]{1,2,0:T(1,128)S(1)} %get-tuple-element.11), channel_id=1, replica_groups=mesh['kv_0'=8,'kv_1'=8,'kv_2'=2,'tp'=4] {'kv_0'}, dimensions={0}, use_global_device_ids=true | all-gather | bytes 288 | tf_op jit(solution)/shard_map/all_gather | solution.py:29
  76.4 0.7 fusion.5
  77.1 2.0 %fusion.9 = f32[8,1,128]{2,1,0:T(1,128)S(1)} fusion(bf16[8,1024,128]{2,1,0:T(8,128)(2,1)} %param.14, bf16[8,1024,1]{1,0,2:T(8,128)(2,1)S(1)} %fusion.5), kind=kOutput, calls=%fused_computation.15 | convolution fusion | flops 2097152 | bytes 2117632 | tf_op jit(solution)/shard_map/bhp,bphd->bhd/dot_general | solution.py:82
  79.1 0.1 exponential_bitcast_fusion
  79.2 0.1 multiply_bitcast_fusion
  79.3 12.1 %psum.69 = f32[8,1,128]{2,0,1:T(8,128)S(1)} all-reduce(f32[8,1,128]{2,0,1:T(8,128)S(1)} %multiply_bitcast_fusion), channel_id=1, replica_groups=mesh['kv_0'=8,'kv_1'=8,'kv_2'=2,'tp'=4] {'kv_0'}, use_global_device_ids=true, to_apply=%region_8.9 | all-reduce | flops 1024 | bytes 8192 | tf_op jit(solution)/shard_map/psum | solution.py:16
  91.4 11.6 %psum.70 = f32[8,1,128]{2,0,1:T(8,128)S(1)} all-reduce(f32[8,1,128]{2,0,1:T(8,128)S(1)} %psum.69), channel_id=1, replica_groups=mesh['kv_0'=8,'kv_1'=8,'kv_2'=2,'tp'=4] {'kv_1'}, use_global_device_ids=true, to_apply=%region_9.10 | all-reduce | flops 1024 | bytes 8192 | tf_op jit(solution)/shard_map/psum | solution.py:16
  103.0 17.5 %psum.71 = f32[8,1,128]{2,0,1:T(8,128)S(1)} all-reduce(f32[8,1,128]{2,0,1:T(8,128)S(1)} %psum.70), channel_id=1, replica_groups=mesh['kv_0'=8,'kv_1'=8,'kv_2'=2,'tp'=4] {'kv_2'}, use_global_device_ids=true, to_apply=%region_10.11 | all-reduce | flops 1024 | bytes 8192 | tf_op jit(solution)/shard_map/psum | solution.py:16
  120.5 0.1 multiply_reduce_fusion
  120.6 0.0 copy-done.2
  120.6 0.0 copy-done.3
  120.6 0.2 convolution_convert_fusion
  120.8 8.0 %all_to_all.5 = bf16[4,8,16]{2,1,0:T(8,128)(2,1)S(1)} all-to-all(bf16[4,8,16]{2,1,0:T(8,128)(2,1)S(1)} %broadcast_in_dim.4), channel_id=1, replica_groups=mesh['kv_0'=8,'kv_1'=8,'kv_2'=2,'tp'=4] {'tp'}, dimensions={0} | all-to-all | bytes 2048 | tf_op jit(solution)/shard_map/all_to_all | solution.py:41
  128.8 0.6 reduce_sum.42
  (6 shorter events, 0.0 us)
Async XLA Ops:
  0.0 47.5 %copy-start = (bf16[8,1024,128]{2,1,0:T(8,128)(2,1)S(1)}, bf16[8,1024,128]{2,1,0:T(8,128)(2,1)}, u32[]{:S(2)}) copy-start(bf16[8,1024,128]{2,1,0:T(8,128)(2,1)} %param.13) | copy-start | bytes 6291460
  0.0 50.2 %copy-start.1 = (s32[8]{0:T(128)S(1)}, s32[8]{0:T(128)}, u32[]{:S(2)}) copy-start(s32[8]{0:T(128)} %param.15) | copy-start | bytes 100
  48.1 72.5 %copy-start.2 = (bf16[128,16]{0,1:T(8,128)(2,1)S(1)}, bf16[128,16]{0,1:T(8,128)(2,1)}, u32[]{:S(2)}) copy-start(bf16[128,16]{0,1:T(8,128)(2,1)} %param.17) | copy-start | bytes 12292
  48.1 72.5 %copy-start.3 = (f32[128]{0:T(128)S(1)}, f32[128]{0:T(128)}, u32[]{:S(2)}) copy-start(f32[128]{0:T(128)} %param.16) | copy-start | bytes 1540
where the time goes:
time: 130 us; the launch traced here: 129 us
  blocking collectives  118 us (91%)
  matrix products  4.37 us (3%)
  local copies, waits for them, and re-layouts  3 us (2%)
  other arithmetic  2.34 us (2%)
  between operations  2.13 us (2%)
    psum x6, blocking collectives, one_axis_at_a_time(): shard = lax.psum(shard, axis)  86.1 us
    unnamed x2, blocking collectives  13.6 us
    all_gather x1, blocking collectives, entering(): pieces = lax.all_gather(so_far, axis)  9.82 us
    all_to_all x1, blocking collectives, copy_for_each(): lax.all_to_all(jnp.broadcast_to(shard[None], (length, *shard.shape)), axi...  7.97 us
    unnamed x13, local copies, waits for them, and re-layouts  2.99 us

commit v1 on v0

v1 whole, which is shorter than its diff:
```python
import functools

import jax
import jax.numpy as jnp
from jax import lax
from jax.experimental import pallas as pl
from jax.experimental.pallas import tpu as pltpu
from jax.sharding import PartitionSpec as P

MESH = pl.DeviceIdType.MESH
D = 2048
EPS = 1e-06
SEQS = 8
DH = 128
SEG = 1024
CHUNKS = SEG // 128
RING = 8
OFFSETS = (4, 3, 5, 2, 6, 1, 7, 0)
F32 = jnp.float32
BF16 = jnp.bfloat16


def kernel(
    tokens_hbm, gain_hbm, wq_hbm, bias_ref, keys_hbm, values_hbm, lengths_ref, head_gain_hbm, wout_hbm,
    out_ref,
    tokens_v, gain_v, wq_v, keys_v, values_v, head_gain_v, wout_v,
    send_a1, recv_a1, recv_a2, send_b1, recv_b1, recv_b2, recv_c,
    load_sems, key_sems, value_sems,
    a1_s, a1_r, a2_s, a2_r, b1_s, b1_r, b2_s, b2_r, c_s, c_r,
):
    kv = lax.axis_index("kv")
    tp = lax.axis_index("tp")
    z, y, core = kv // 16, (kv // 2) % 8, kv % 2

    def at(zz, yy, cc, xx):
        return {"kv": (zz * 8 + yy) * 2 + cc, "tp": xx}

    y_peers = [(2 * dy + dc, (y + dy) % 8, (core + dc) % 2) for dy in OFFSETS for dc in (0, 1) if dy or dc]
    z_peers = [(2 * dz + dc, (z + dz) % 8, (core + dc) % 2) for dz in OFFSETS for dc in (0, 1) if dz or dc]

    barrier = pltpu.get_barrier_semaphore()
    for k, yy, cc in y_peers:
        pl.semaphore_signal(barrier, inc=1, device_id=at(z, yy, cc, tp), device_id_type=MESH)
    for k, zz, cc in z_peers:
        if k > 1:
            pl.semaphore_signal(barrier, inc=1, device_id=at(zz, y, cc, tp), device_id_type=MESH)
    for dx in (2, 1, 3):
        pl.semaphore_signal(barrier, inc=1, device_id=at(z, y, core, (tp + dx) % 4), device_id_type=MESH)

    small = [
        pltpu.make_async_copy(src, dst, load_sems.at[i])
        for i, (src, dst) in enumerate(
            [(tokens_hbm, tokens_v), (gain_hbm, gain_v), (wq_hbm, wq_v), (head_gain_hbm, head_gain_v), (wout_hbm, wout_v)]
        )
    ]
    for copy in small:
        copy.start()
    key_copies = [pltpu.make_async_copy(keys_hbm.at[b], keys_v.at[b], key_sems.at[b]) for b in range(SEQS)]
    value_copies = [pltpu.make_async_copy(values_hbm.at[b], values_v.at[b], value_sems.at[b]) for b in range(SEQS)]
    for copy in key_copies + value_copies:
        copy.start()

    row = lax.broadcasted_iota(jnp.int32, (8, 128), 0)
    upper = row < 4

    def swap(tile):
        return pltpu.roll(tile, 4, 0)

    def halves(full, scalars):
        return jnp.where(upper, full, swap(scalars)), jnp.where(upper, swap(full), scalars)

    def joined(first, second):
        return jnp.where(upper, first, swap(second)), jnp.where(upper, swap(first), second)

    def scatter_y(src, dst, s_sems, r_sems):
        copies = []
        for k, yy, cc in y_peers:
            copies.append(
                pltpu.make_async_remote_copy(
                    src_ref=src.at[cc], dst_ref=dst.at[y * 2 + core], send_sem=s_sems.at[k], recv_sem=r_sems.at[k],
                    device_id=at(z, yy, cc, tp), device_id_type=MESH,
                )
            )
            copies[-1].start()
        return copies

    def spread_z(dst, s_sems, r_sems):
        copies = []
        for k, zz, cc in z_peers:
            copies.append(
                pltpu.make_async_remote_copy(
                    src_ref=dst.at[z * 2 + core], dst_ref=dst.at[z * 2 + core], send_sem=s_sems.at[k],
                    recv_sem=r_sems.at[k], device_id=at(zz, y, cc, tp), device_id_type=MESH,
                )
            )
            copies[-1].start()
        return copies

    for copy in small[:3]:
        copy.wait()
    as_float = tokens_v[...].astype(F32)
    gained = (as_float * gain_v[...]).astype(BF16)
    partial = jnp.dot(gained, wq_v[...], preferred_element_type=F32)
    squares = jnp.broadcast_to(jnp.sum(as_float * as_float, axis=1, keepdims=True), (8, 128))
    first, second = halves(partial, squares)
    send_a1[0] = first
    send_a1[1] = second
    recv_a1[y * 2 + core] = jnp.where(core == 0, first, second)
    pl.semaphore_wait(barrier, 32)
    copies_a1 = scatter_y(send_a1, recv_a1, a1_s, a1_r)
    for copy in copies_a1:
        copy.wait_recv()
    recv_a2[z * 2 + core] = jnp.sum(recv_a1[...], axis=0)
    copies_a2 = spread_z(recv_a2, a2_s, a2_r)

    r_iota = lax.broadcasted_iota(jnp.int32, (128, 256), 0)
    s_iota = lax.broadcasted_iota(jnp.int32, (128, 256), 1)
    after = jnp.where((r_iota > s_iota) | (s_iota >= 128), 1.0, 0.0).astype(BF16)
    length = jnp.zeros((8, 128), jnp.int32)
    for b in range(SEQS):
        length = jnp.where(row == b, lengths_ref[b], length)
    bias = bias_ref[0]
    for copy in key_copies:
        copy.wait()

    for copy in copies_a2:
        copy.wait_recv()
    by_core = jnp.sum(recv_a2[...].reshape(8, 2, 8, 128), axis=0)
    summed, total_sq = joined(by_core[0], by_core[1])
    query = (summed * lax.rsqrt(total_sq / D + EPS)).astype(BF16)

    dims = (((1,), (1,)), ((), ()))
    raw = [None] * CHUNKS
    for b in range(SEQS):
        got = lax.dot_general(query, keys_v[b], dims, preferred_element_type=F32)
        for n in range(CHUNKS):
            piece = got[:, n * 128 : (n + 1) * 128]
            raw[n] = piece if b == 0 else jnp.where(row == b, piece, raw[n])
    lane = lax.broadcasted_iota(jnp.int32, (8, 128), 1)
    log_gate, log_keep, usable = [], [], []
    for n in range(CHUNKS):
        score = raw[n] * DH**-0.5 + bias
        tail = jnp.log1p(jnp.exp(-jnp.abs(score)))
        ok = lane + (kv * SEG + n * 128) < length
        usable.append(ok)
        log_gate.append(jnp.minimum(score, 0.0) - tail)
        log_keep.append(jnp.where(ok, -jnp.maximum(score, 0.0) - tail, 0.0))
    keep = jnp.concatenate(log_keep, axis=0)
    high = keep.astype(BF16)
    rest = keep - high.astype(F32)
    mid = rest.astype(BF16)
    low = (rest - mid.astype(F32)).astype(BF16)
    sums = jnp.dot(jnp.concatenate([high, mid, low], axis=0), after, preferred_element_type=F32)
    sums = sums[0:64] + sums[64:128] + sums[128:192]
    later = jnp.zeros((8, 128), F32)
    pieces = [None] * CHUNKS
    for n in reversed(range(CHUNKS)):
        inside = sums[n * 8 : n * 8 + 8, 0:128]
        pieces[n] = jnp.where(usable[n], jnp.exp(log_gate[n] + (inside + later)), 0.0).astype(BF16)
        later = later + sums[n * 8 : n * 8 + 8, 128:256]
    weights = jnp.concatenate(pieces, axis=1)
    for copy in value_copies:
        copy.wait()
    local = None
    for b in range(SEQS):
        got = jnp.dot(weights, values_v[b], preferred_element_type=F32)
        local = got if b == 0 else jnp.where(row == b, got, local)

    first, second = halves(local, later)
    send_b1[0] = first
    send_b1[1] = second
    recv_b1[y * 2 + core] = jnp.where(core == 0, first, second)
    copies_b1 = scatter_y(send_b1, recv_b1, b1_s, b1_r)
    for copy in copies_b1:
        copy.wait_recv()
    later = jnp.zeros((8, 128), F32)
    total = jnp.zeros((8, 128), F32)
    for i in reversed(range(16)):
        tile = recv_b1[i]
        total = total + tile * jnp.exp(swap(jnp.where(upper, 0.0, later)))
        later = later + tile
    recv_b2[z * 2 + core] = jnp.where(upper, total, later)
    copies_b2 = spread_z(recv_b2, b2_s, b2_r)
    for copy in small[3:]:
        copy.wait()
    for copy in copies_b2:
        copy.wait_recv()
    later = jnp.zeros((8, 128), F32)
    attended = jnp.zeros((8, 128), F32)
    for i in reversed(range(8)):
        outs, totals = joined(recv_b2[2 * i], recv_b2[2 * i + 1])
        attended = attended + outs * jnp.exp(later)
        later = later + totals

    mean_sq = jnp.sum(attended * attended, axis=1, keepdims=True) / DH
    normed = (attended * lax.rsqrt(mean_sq + EPS) * head_gain_v[...]).astype(BF16)
    part = lax.dot_general(normed, wout_v[...], dims, preferred_element_type=F32)
    recv_c[tp] = part.astype(BF16)
    copies_c = []
    for k, dx in enumerate((2, 1, 3)):
        copies_c.append(
            pltpu.make_async_remote_copy(
                src_ref=recv_c.at[tp], dst_ref=recv_c.at[tp], send_sem=c_s.at[k], recv_sem=c_r.at[k],
                device_id=at(z, y, core, (tp + dx) % 4), device_id_type=MESH,
            )
        )
        copies_c[-1].start()
    for copy in copies_a1 + copies_a2 + copies_b1 + copies_b2:
        copy.wait_send()
    for copy in copies_c:
        copy.wait()
    mixed = recv_c[0].astype(F32)
    for i in range(1, 4):
        mixed = mixed + recv_c[i].astype(F32)
    out_ref[...] = mixed.astype(BF16)


def shards(tokens, in_gain, w_query, score_bias, cache_keys, cache_values, lengths, head_gain, w_out):
    dma = pltpu.SemaphoreType.DMA
    any_space = pl.BlockSpec(memory_space=pl.ANY)
    smem = pl.BlockSpec(memory_space=pltpu.SMEM)
    return pl.pallas_call(
        kernel,
        out_shape=jax.ShapeDtypeStruct((SEQS, 16), BF16),
        in_specs=[any_space, any_space, any_space, smem, any_space, any_space, smem, any_space, any_space],
        out_specs=pl.BlockSpec(memory_space=pltpu.VMEM),
        scratch_shapes=[
            pltpu.VMEM((SEQS, 16), BF16),
            pltpu.VMEM((1, 16), F32),
            pltpu.VMEM((16, DH), BF16),
            pltpu.VMEM((SEQS, SEG, DH), BF16),
            pltpu.VMEM((SEQS, SEG, DH), BF16),
            pltpu.VMEM((1, DH), F32),
            pltpu.VMEM((16, DH), BF16),
            pltpu.VMEM((2, 8, 128), F32),
            pltpu.VMEM((16, 8, 128), F32),
            pltpu.VMEM((16, 8, 128), F32),
            pltpu.VMEM((2, 8, 128), F32),
            pltpu.VMEM((16, 8, 128), F32),
            pltpu.VMEM((16, 8, 128), F32),
            pltpu.VMEM((4, SEQS, 16), BF16),
            dma((5,)),
            dma((SEQS,)),
            dma((SEQS,)),
            dma((16,)),
            dma((16,)),
            dma((16,)),
            dma((16,)),
            dma((16,)),
            dma((16,)),
            dma((16,)),
            dma((16,)),
            dma((3,)),
            dma((3,)),
        ],
        compiler_params=pltpu.CompilerParams(collective_id=0, has_side_effects=True),
        name="decode",
    )(
        tokens, in_gain.reshape(1, 16), w_query, score_bias, cache_keys, cache_values, lengths,
        head_gain.reshape(1, DH), w_out.T,
    )


def solution(mesh):
    placed = (
        P(None, "kv"), P("kv"), P("kv", "tp"), P("tp"), P(None, "kv", "tp"), P(None, "kv", "tp"), P(), P("tp"),
        P("tp", "kv"),
    )
    return jax.shard_map(shards, mesh=mesh, in_specs=placed, out_specs=P(None, "kv"), check_vma=False)
```

time: 130 us -> 43 us (0.33)
  blocking collectives: 118 us -> 0 us
  Pallas kernels: 0 us -> 40.9 us
  matrix products: 4.37 us -> 0 us
  other arithmetic: 2.34 us -> 0 us
  local copies, waits for them, and re-layouts: 3 us -> 1.26 us
  between operations: 2.13 us -> 0.66 us
    psum x6 -> x0, blocking collectives: 86.1 us -> none  [one_axis_at_a_time(): shard = lax.psum(shard, axis)]
    pallas_call x0 -> x1, Pallas kernels: none -> 40.9 us  [shards(): pl.pallas_call(kernel, out_shape=jax.ShapeDtypeStruct((SEQS, 16), BF16),...]
    unnamed x2 -> x0, blocking collectives: 13.6 us -> none
    all_gather x1 -> x0, blocking collectives: 9.82 us -> none  [entering(): pieces = lax.all_gather(so_far, axis)]
    all_to_all x1 -> x0, blocking collectives: 7.97 us -> none  [copy_for_each(): lax.all_to_all(jnp.broadcast_to(shard[None], (length, *shard.shape)), axi...]
    dot_general x5 -> x0, matrix products: 4.37 us -> none  [the longest x1 1.98 us: shards(): jnp.einsum('bhp,bphd->bhd', weights, value_heads, preferred_element_type=...]
    reduce_sum x4 -> x0, other arithmetic: 1.84 us -> none  [the longest x1 0.94 us: shards(): squares = jnp.sum(as_float * as_float, axis=1)]
    unnamed x13 -> x1, local copies, waits for them, and re-layouts: 2.99 us -> 1.26 us
where the time goes in v1:
time: 43 us; the launch traced here: 42.8 us
  Pallas kernels  40.9 us (95%)
  local copies, waits for them, and re-layouts  1.26 us (3%)
  between operations  0.66 us (2%)
    pallas_call x1, Pallas kernels, shards(): pl.pallas_call(kernel, out_shape=jax.ShapeDtypeStruct((SEQS, 16), BF16),...  40.9 us
    unnamed x1, local copies, waits for them, and re-layouts  1.26 us

profile of v1, /device:TPU:1, one launch (start us, length us, event | category | flops | bytes accessed | tf_op | source)
XLA Modules:
  0.0 42.8 jit_solution(4850803889190742416)
XLA Ops:
  0.7 40.9 %decode.1 = bf16[8,16]{1,0:T(8,128)(2,1)} custom-call(bf16[8,16]{1,0:T(8,128)(2,1)} %tokens_hbm.1, f32[1,16]{1,0:T(1,128)} %bitcast.4, bf16[16,128]{1,0:T(8,128)(2,1)} %wq_hbm.1, f32[1]{0:T(128)S(6)} %copy.11.bias_ref, bf16[8,1024,128]{2,1,0:T(8,128)(2,1)} %keys_hbm.1, bf16[8,1024,128]{2,1,0:T(8,128)(2,1)} %values_hbm.1, s32[8]{0:T(128)} %lengths_ref.1, ...), custom_call_target="tpu_custom_call" | custom-call | tf_op jit(solution)/shard_map/decode/pallas_call | solution.py:222
  41.6 1.3 %copy.12 = bf16[8,16]{1,0:T(8,128)(2,1)} copy(bf16[8,16]{1,0:T(8,128)(2,1)} %decode.1) | data formatting | bytes 512

commit v2 on v1

v2 whole, which is shorter than its diff:
```python
import jax
import jax.numpy as jnp
from jax import lax
from jax.experimental import pallas as pl
from jax.experimental.pallas import tpu as pltpu
from jax.sharding import PartitionSpec as P

MESH = pl.DeviceIdType.MESH
D = 2048
EPS = 1e-06
SEQS = 8
DH = 128
SEG = 1024
CHUNKS = SEG // 128
COLS = 16
OFFSETS = (4, 3, 5, 2, 6, 1, 7)
F32 = jnp.float32
BF16 = jnp.bfloat16
DIMS = (((1,), (1,)), ((), ()))


def kernel(
    tokens_hbm, gain_hbm, wq_hbm, bias_ref, keys_hbm, values_hbm, lengths_ref, head_gain_hbm, wout_hbm,
    out_ref,
    tokens_v, gain_v, wq_v, keys_v, values_v, head_gain_v, wout_v,
    sum_y, sum_z, total_y, total_z, local_y, local_z, parts, parts_0,
    load_sems, key_sems, value_sems, wout_s, wout_r,
    sum_y_s, sum_y_r, sum_z_s, sum_z_r, total_y_s, total_y_r, total_z_s, total_z_r,
    local_y_s, local_y_r, local_z_s, local_z_r, parts_s, parts_r,
):
    kv = lax.axis_index("kv")
    tp = lax.axis_index("tp")
    z, y, core = kv // 16, (kv // 2) % 8, kv % 2
    adder = core == 1
    mine = y * 2 + core

    def at(zz, yy, cc, xx):
        return {"kv": (zz * 8 + yy) * 2 + cc, "tp": xx}

    def signal(zz, yy, cc, xx):
        pl.semaphore_signal(barrier, inc=1, device_id=at(zz, yy, cc, xx), device_id_type=MESH)

    def send(src, dst, s_sem, r_sem, zz, yy, cc, xx):
        copy = pltpu.make_async_remote_copy(
            src_ref=src, dst_ref=dst, send_sem=s_sem, recv_sem=r_sem, device_id=at(zz, yy, cc, xx), device_id_type=MESH
        )
        copy.start()

    def waiter(dst, s_sem, r_sem):
        return pltpu.make_async_remote_copy(
            src_ref=dst, dst_ref=dst, send_sem=s_sem, recv_sem=r_sem, device_id=at(z, y, 1 - core, tp), device_id_type=MESH
        )

    barrier = pltpu.get_barrier_semaphore()

    @pl.when(adder)
    def _():
        for d in OFFSETS:
            for cc in (0, 1):
                signal(z, (y + d) % 8, cc, tp)
            signal((z + d) % 8, y, 1, tp)
        for d in (2, 1, 3):
            signal(z, y, 1, (tp + d) % 4)
        signal(z, y, 0, tp)

    @pl.when(core == 0)
    def _():
        for d in OFFSETS:
            signal((z + d) % 8, y, 1, tp)
        for d in (2, 1, 3):
            signal(z, y, 1, (tp + d) % 4)
        signal(z, y, 1, tp)

    small = [
        pltpu.make_async_copy(src, dst, load_sems.at[i])
        for i, (src, dst) in enumerate(
            [(tokens_hbm, tokens_v), (gain_hbm, gain_v), (wq_hbm, wq_v), (head_gain_hbm, head_gain_v),
             (wout_hbm, wout_v.at[core])]
        )
    ]
    for copy in small:
        copy.start()
    key_copies = [pltpu.make_async_copy(keys_hbm.at[b], keys_v.at[b], key_sems.at[b]) for b in range(SEQS)]
    value_copies = [pltpu.make_async_copy(values_hbm.at[b], values_v.at[b], value_sems.at[b]) for b in range(SEQS)]
    for copy in key_copies + value_copies:
        copy.start()

    row = lax.broadcasted_iota(jnp.int32, (8, 128), 0)
    lane = lax.broadcasted_iota(jnp.int32, (8, 128), 1)

    def to_adders(buf, s_sems, r_sems):
        for d in OFFSETS:
            send(buf.at[mine], buf.at[mine], s_sems.at[d], r_sems.at[2 * ((8 - d) % 8) + core], z, (y + d) % 8, 1, tp)

        @pl.when(core == 0)
        def _():
            send(buf.at[mine], buf.at[mine], s_sems.at[0], r_sems.at[0], z, y, 1, tp)

    def from_line(buf, s_sems, r_sems):
        for d in OFFSETS:
            for cc in (0, 1):
                waiter(buf.at[mine], s_sems.at[0], r_sems.at[2 * d + cc]).wait_recv()
        waiter(buf.at[mine], s_sems.at[0], r_sems.at[0]).wait_recv()

    def sent_to_adders(buf, s_sems, r_sems):
        for d in OFFSETS:
            waiter(buf.at[mine], s_sems.at[d], r_sems.at[0]).wait_send()

        @pl.when(core == 0)
        def _():
            waiter(buf.at[mine], s_sems.at[0], r_sems.at[0]).wait_send()

    for copy in small[:3]:
        copy.wait()
    as_float = tokens_v[...].astype(F32)
    gained = (as_float * gain_v[...]).astype(BF16)
    partial = jnp.dot(gained, wq_v[...], preferred_element_type=F32)
    squares = jnp.sum(as_float * as_float, axis=1, keepdims=True)
    sum_y[mine, 0:8] = partial
    sum_y[mine, 8:9] = jnp.sum(jnp.where(row == lane, squares, 0.0), axis=0, keepdims=True)

    @pl.when(adder)
    def _():
        pl.semaphore_wait(barrier, 28)

    @pl.when(core == 0)
    def _():
        pl.semaphore_wait(barrier, 8)

    to_adders(sum_y, sum_y_s, sum_y_r)

    @pl.when(core == 0)
    def _():
        small[4].wait()
        send(wout_v.at[0], wout_v.at[0], wout_s, wout_r, z, y, 1, tp)

    @pl.when(adder)
    def _():
        from_line(sum_y, sum_y_s, sum_y_r)
        sum_z[z] = jnp.sum(sum_y[...], axis=0)
        for d in OFFSETS:
            for cc in (0, 1):
                send(sum_z.at[z], sum_z.at[z], sum_z_s.at[2 * d + cc], sum_z_r.at[(8 - d) % 8], (z + d) % 8, y, cc, tp)
        send(sum_z.at[z], sum_z.at[z], sum_z_s.at[0], sum_z_r.at[0], z, y, 0, tp)

    r_iota = lax.broadcasted_iota(jnp.int32, (128, 256), 0)
    s_iota = lax.broadcasted_iota(jnp.int32, (128, 256), 1)
    after = jnp.where((r_iota > s_iota) | (s_iota >= 128), 1.0, 0.0).astype(BF16)
    length = jnp.zeros((8, 128), jnp.int32)
    for b in range(SEQS):
        length = jnp.where(row == b, lengths_ref[b], length)
    bias = bias_ref[0]
    for copy in key_copies + value_copies:
        copy.wait()

    for d in OFFSETS:
        waiter(sum_z.at[z], sum_z_s.at[0], sum_z_r.at[d]).wait_recv()

    @pl.when(core == 0)
    def _():
        waiter(sum_z.at[z], sum_z_s.at[0], sum_z_r.at[0]).wait_recv()

    summed = jnp.sum(sum_z[...], axis=0)
    total_sq = jnp.sum(jnp.where(row == lane, summed[8:9], 0.0), axis=1, keepdims=True)
    query = (summed[0:8] * lax.rsqrt(total_sq / D + EPS)).astype(BF16)

    raw = [None] * CHUNKS
    for b in range(SEQS):
        got = lax.dot_general(query, keys_v[b], DIMS, preferred_element_type=F32)
        for n in range(CHUNKS):
            piece = got[:, n * 128 : (n + 1) * 128]
            raw[n] = piece if b == 0 else jnp.where(row == b, piece, raw[n])
    log_gate, log_keep, usable = [], [], []
    for n in range(CHUNKS):
        score = raw[n] * DH**-0.5 + bias
        tail = jnp.log1p(jnp.exp(-jnp.abs(score)))
        ok = lane + (kv * SEG + n * 128) < length
        usable.append(ok)
        log_gate.append(jnp.minimum(score, 0.0) - tail)
        log_keep.append(jnp.where(ok, -jnp.maximum(score, 0.0) - tail, 0.0))
    keep = jnp.concatenate(log_keep, axis=0)
    high = keep.astype(BF16)
    rest = keep - high.astype(F32)
    mid = rest.astype(BF16)
    low = (rest - mid.astype(F32)).astype(BF16)
    sums = jnp.dot(jnp.concatenate([high, mid, low], axis=0), after, preferred_element_type=F32)
    sums = sums[0:64] + sums[64:128] + sums[128:192]
    later = jnp.zeros((8, 128), F32)
    pieces = [None] * CHUNKS
    for n in reversed(range(CHUNKS)):
        inside = sums[n * 8 : n * 8 + 8, 0:128]
        pieces[n] = jnp.where(usable[n], jnp.exp(log_gate[n] + (inside + later)), 0.0).astype(BF16)
        later = later + sums[n * 8 : n * 8 + 8, 128:256]
    total_y[mine] = later
    to_adders(total_y, total_y_s, total_y_r)
    weights = jnp.concatenate(pieces, axis=1)
    local = None
    for b in range(SEQS):
        got = jnp.dot(weights, values_v[b], preferred_element_type=F32)
        local = got if b == 0 else jnp.where(row == b, got, local)
    local_y[mine] = local
    to_adders(local_y, local_y_s, local_y_r)

    @pl.when(adder)
    def _():
        from_line(total_y, total_y_s, total_y_r)
        later = jnp.zeros((8, 128), F32)
        fade = [None] * 16
        for i in reversed(range(16)):
            fade[i] = jnp.exp(later)
            later = later + total_y[i]
        total_z[z] = later
        for d in OFFSETS:
            send(total_z.at[z], total_z.at[z], total_z_s.at[d], total_z_r.at[(8 - d) % 8], (z + d) % 8, y, 1, tp)
        from_line(local_y, local_y_s, local_y_r)
        terms = [local_y[i] * fade[i] for i in range(16)]
        while len(terms) > 1:
            terms = [a + b for a, b in zip(terms[::2], terms[1::2])]
        local_z[z] = terms[0]
        for d in OFFSETS:
            send(local_z.at[z], local_z.at[z], local_z_s.at[d], local_z_r.at[(8 - d) % 8], (z + d) % 8, y, 1, tp)
        for copy in small[3:]:
            copy.wait()
        waiter(wout_v.at[0], wout_s, wout_r).wait_recv()
        for d in OFFSETS:
            waiter(total_z.at[z], total_z_s.at[0], total_z_r.at[d]).wait_recv()
        later = jnp.zeros((8, 128), F32)
        fade = [None] * 8
        for i in reversed(range(8)):
            fade[i] = jnp.exp(later)
            later = later + total_z[i]
        for d in OFFSETS:
            waiter(local_z.at[z], local_z_s.at[0], local_z_r.at[d]).wait_recv()
        terms = [local_z[i] * fade[i] for i in range(8)]
        while len(terms) > 1:
            terms = [a + b for a, b in zip(terms[::2], terms[1::2])]
        attended = terms[0]
        mean_sq = jnp.sum(attended * attended, axis=1, keepdims=True) / DH
        normed = (attended * lax.rsqrt(mean_sq + EPS) * head_gain_v[...]).astype(BF16)
        parts[tp] = lax.dot_general(normed, wout_v[1], DIMS, preferred_element_type=F32).astype(BF16)
        parts_0[...] = lax.dot_general(normed, wout_v[0], DIMS, preferred_element_type=F32).astype(BF16)
        for d in (2, 1, 3):
            send(parts_0, parts.at[tp], parts_s.at[d], parts_r.at[4 - d], z, y, 0, (tp + d) % 4)
            send(parts.at[tp], parts.at[tp], parts_s.at[4 + d], parts_r.at[4 - d], z, y, 1, (tp + d) % 4)
        send(parts_0, parts.at[tp], parts_s.at[0], parts_r.at[0], z, y, 0, tp)

    sent_to_adders(sum_y, sum_y_s, sum_y_r)
    sent_to_adders(total_y, total_y_s, total_y_r)
    sent_to_adders(local_y, local_y_s, local_y_r)

    @pl.when(adder)
    def _():
        for d in OFFSETS:
            for cc in (0, 1):
                waiter(sum_z.at[z], sum_z_s.at[2 * d + cc], sum_z_r.at[0]).wait_send()
            waiter(total_z.at[z], total_z_s.at[d], total_z_r.at[0]).wait_send()
            waiter(local_z.at[z], local_z_s.at[d], local_z_r.at[0]).wait_send()
        waiter(sum_z.at[z], sum_z_s.at[0], sum_z_r.at[0]).wait_send()
        for d in (2, 1, 3):
            for first in (0, 4):
                waiter(parts.at[tp], parts_s.at[first + d], parts_r.at[0]).wait_send()
        waiter(parts.at[tp], parts_s.at[0], parts_r.at[0]).wait_send()

    @pl.when(core == 0)
    def _():
        waiter(wout_v.at[0], wout_s, wout_r).wait_send()
        small[3].wait()
        waiter(parts.at[tp], parts_s.at[0], parts_r.at[0]).wait_recv()

    for d in (2, 1, 3):
        waiter(parts.at[tp], parts_s.at[0], parts_r.at[d]).wait_recv()
    mixed = parts[0].astype(F32)
    for i in range(1, 4):
        mixed = mixed + parts[i].astype(F32)
    out_ref[...] = mixed.astype(BF16)


def shards(tokens, in_gain, w_query, score_bias, cache_keys, cache_values, lengths, head_gain, w_out):
    dma = pltpu.SemaphoreType.DMA
    any_space = pl.BlockSpec(memory_space=pl.ANY)
    smem = pl.BlockSpec(memory_space=pltpu.SMEM)
    return pl.pallas_call(
        kernel,
        out_shape=jax.ShapeDtypeStruct((SEQS, COLS), BF16),
        in_specs=[any_space, any_space, any_space, smem, any_space, any_space, smem, any_space, any_space],
        out_specs=pl.BlockSpec(memory_space=pltpu.VMEM),
        scratch_shapes=[
            pltpu.VMEM((SEQS, 16), BF16),
            pltpu.VMEM((1, 16), F32),
            pltpu.VMEM((16, DH), BF16),
            pltpu.VMEM((SEQS, SEG, DH), BF16),
            pltpu.VMEM((SEQS, SEG, DH), BF16),
            pltpu.VMEM((1, DH), F32),
            pltpu.VMEM((2, COLS, DH), BF16),
            pltpu.VMEM((16, 9, 128), F32),
            pltpu.VMEM((8, 9, 128), F32),
            pltpu.VMEM((16, 8, 128), F32),
            pltpu.VMEM((8, 8, 128), F32),
            pltpu.VMEM((16, 8, 128), F32),
            pltpu.VMEM((8, 8, 128), F32),
            pltpu.VMEM((4, SEQS, COLS), BF16),
            pltpu.VMEM((SEQS, COLS), BF16),
            dma((5,)),
            dma((SEQS,)),
            dma((SEQS,)),
            dma,
            dma,
            dma((8,)), dma((16,)), dma((16,)), dma((8,)),
            dma((8,)), dma((16,)), dma((8,)), dma((8,)),
            dma((8,)), dma((16,)), dma((8,)), dma((8,)),
            dma((8,)), dma((4,)),
        ],
        compiler_params=pltpu.CompilerParams(collective_id=0, has_side_effects=True),
        name="decode",
    )(
        tokens, in_gain.reshape(1, 16), w_query, score_bias, cache_keys, cache_values, lengths,
        head_gain.reshape(1, DH), w_out.T,
    )


def solution(mesh):
    placed = (
        P(None, "kv"), P("kv"), P("kv", "tp"), P("tp"), P(None, "kv", "tp"), P(None, "kv", "tp"), P(), P("tp"),
        P("tp", "kv"),
    )
    return jax.shard_map(shards, mesh=mesh, in_specs=placed, out_specs=P(None, "kv"), check_vma=False)
```

time: 43 us -> 40.6 us (0.944)
  Pallas kernels: 40.9 us -> 38.5 us
    pallas_call x1, Pallas kernels: 40.9 us -> 38.5 us  [shards(): pl.pallas_call(kernel, out_shape=jax.ShapeDtypeStruct((SEQS, COLS), BF16)...]
where the time goes in v2:
time: 40.6 us; the launch traced here: 40.4 us
  Pallas kernels  38.5 us (95%)
  local copies, waits for them, and re-layouts  1.26 us (3%)
  between operations  0.66 us (2%)
    pallas_call x1, Pallas kernels, shards(): pl.pallas_call(kernel, out_shape=jax.ShapeDtypeStruct((SEQS, COLS), BF16)...  38.5 us
    unnamed x1, local copies, waits for them, and re-layouts  1.26 us

profile of v2, /device:TPU:1, one launch (start us, length us, event | category | flops | bytes accessed | tf_op | source)
XLA Modules:
  0.0 40.4 jit_solution(4287604098941381960)
XLA Ops:
  0.7 38.5 %decode.1 = bf16[8,16]{1,0:T(8,128)(2,1)} custom-call(bf16[8,16]{1,0:T(8,128)(2,1)} %tokens_hbm.1, f32[1,16]{1,0:T(1,128)} %bitcast.4, bf16[16,128]{1,0:T(8,128)(2,1)} %wq_hbm.1, f32[1]{0:T(128)S(6)} %copy.11.bias_ref, bf16[8,1024,128]{2,1,0:T(8,128)(2,1)} %keys_hbm.1, bf16[8,1024,128]{2,1,0:T(8,128)(2,1)} %values_hbm.1, s32[8]{0:T(128)} %lengths_ref.1, ...), custom_call_target="tpu_custom_call" | custom-call | tf_op jit(solution)/shard_map/decode/pallas_call | solution.py:282
  39.2 1.3 %copy.12 = bf16[8,16]{1,0:T(8,128)(2,1)} copy(bf16[8,16]{1,0:T(8,128)(2,1)} %decode.1) | data formatting | bytes 512
